TPU v7x, 32 devices: a whole 2x2x4 slice. The times are simulated.
32 devices in a mesh: sp: 4 (over z), fs: 4 (over y, core), tp: 2 (over x).
Axes of the slice: x: 2, y: 2, z: 4, core: 2. Of those that a mesh axis runs over, the one named last changes fastest.
Arguments:
- input_layer_rows: bfloat16 [4, 1024, 2048], P('fs', 'sp'), may hold values from -6 to 6
- input_norm_gain: float32 [2048], replicated, may hold values from 0.1 to 1.9
- query_weight_attention: bfloat16 [2048, 1024], P(('sp', 'fs'), 'tp'), may hold values from -0.125 to 0.125
- key_weight_attention: bfloat16 [2048, 1024], P(('sp', 'fs'), 'tp'), may hold values from -0.125 to 0.125
- value_weight_attention: bfloat16 [2048, 1024], P(('sp', 'fs'), 'tp'), may hold values from -0.125 to 0.125
- query_weight_recurrent: bfloat16 [2048, 1024], P(('sp', 'fs'), 'tp'), may hold values from -0.125 to 0.125
- forget_weight_recurrent: bfloat16 [2048, 1024], P(('sp', 'fs'), 'tp'), may hold values from -0.125 to 0.125
- value_weight_recurrent: bfloat16 [2048, 1024], P(('sp', 'fs'), 'tp'), may hold values from -0.125 to 0.125
- gate_weight_recurrent: bfloat16 [2048, 1024], P(('sp', 'fs'), 'tp'), may hold values from -0.125 to 0.125
- output_weight_attention: bfloat16 [2048, 1024], P(('sp', 'fs'), 'tp'), may hold values from -0.125 to 0.125
- emitted_projection_linear_scan: bfloat16 [2048, 1024], P(('sp', 'fs'), 'tp'), may hold values from -0.125 to 0.125
- score_offset: float32 [8], P('tp'), as said below
- attention_norm_gain: float32 [1024], P('tp'), may hold values from 0.1 to 1.9
- recurrence_norm_gain: float32 [1024], P('tp'), may hold values from 0.1 to 1.9
- forget_floor: float32 [1024], P('tp'), may hold values from 0.1 to 0.5
- forget_offset: float32 [1024], P('tp'), as said below
- extra_log_decay: float32 [4, 1024, 1024], P('fs', 'sp', 'tp')
Outputs:
- layer_out: bfloat16 [4, 1024, 2048], P('fs', ('sp', 'tp'))
- row_log_total: float32 [4, 8, 1024], P('fs', 'tp', 'sp')
Inputs may be any that keep to these rules, and one draw needn't show every extreme that they name: `score_offset`: each head's offset lies between -ln(1024) - 2 and -ln(1024) + 0.5. `forget_offset`: each channel's offset lies between ln(256) - 3 and ln(1024) + 0.6.
All inputs are finite; a program needn't handle non-finite values.
Results may differ from a plain program's by a relative error of at most 0.015.
Values may be sent and summed in bfloat16 or wider, within the bound.
A program may use at most 64 MiB of HBM per device.

v0:
```python
import jax
import jax.numpy as jnp
from jax import lax
from jax.sharding import PartitionSpec as P

HEAD = 128
BLOCK = 64
epsilon = 1e-06
log_floor = 0.05


def entering(shard, axis, combine, identity):
    size, index = (lax.axis_size(axis), lax.axis_index(axis))
    everything = jax.tree.map(
        lambda part, kind: lax.all_gather(part.astype(kind), axis),
        shard,
        (jnp.bfloat16, jnp.bfloat16),
    )
    start = jax.tree.map(
        lambda part, zero: jnp.broadcast_to(jnp.asarray(zero, part.dtype), part.shape),
        shard,
        identity,
    )

    def hop(k, before):
        reached = k < index
        new = combine(
            before, jax.tree.map(lambda part, own: part[k].astype(own.dtype), everything, shard)
        )
        return jax.tree.map(lambda a, b: jnp.where(reached, a, b), new, before)

    return lax.fori_loop(0, size, hop, start)


def head_norm(values, gain):
    square_mean = jnp.mean(values * values, axis=-1, keepdims=True)
    return values * lax.rsqrt(square_mean + epsilon) * gain


def recurrence_block(memory_matrix, inputs):
    query_slice, decay_part, key_slice, value_slice = inputs
    highest_score = lax.Precision.HIGHEST
    length = decay_part.shape[0]
    running_total = jnp.cumsum(decay_part, axis=0)
    causal = (
        lax.broadcasted_iota(jnp.int32, (length, length), 0)
        >= lax.broadcasted_iota(jnp.int32, (length, length), 1)
    )[:, :, None, None]
    relative = jnp.where(causal, running_total[:, None] - running_total[None, :], -jnp.inf)
    pairwise = jnp.sum(query_slice[:, None] * key_slice[None, :] * jnp.exp(relative), axis=-1)
    inner_part = jnp.einsum("tsh,shv->thv", pairwise, value_slice, precision=highest_score)
    carried_state = jnp.einsum(
        "fby,bym->fbm", query_slice * jnp.exp(running_total), memory_matrix, precision=highest_score
    )
    final_total = running_total[-1]
    updated_state = jnp.exp(final_total)[:, :, None] * memory_matrix + jnp.einsum(
        "rxc,rxa->xca",
        key_slice * jnp.exp(final_total[None] - running_total),
        value_slice,
        precision=highest_score,
    )
    return (updated_state, inner_part + carried_state)


def stick_piece(queries, shifts, weighted, keep_total, key_value, is_own, is_valid):
    scores = (
        jnp.einsum("thd,shd->hts", queries, key_value[0], preferred_element_type=jnp.float32)
        * HEAD ** (-0.5)
        + shifts[:, None, None]
    )
    logarithmic_retention = jax.nn.log_sigmoid(-scores)
    if is_own:
        rows_here = scores.shape[1]
        strict = lax.broadcasted_iota(jnp.int32, (rows_here, rows_here), 0) > lax.broadcasted_iota(
            jnp.int32, (rows_here, rows_here), 1
        )
        logarithmic_retention = jnp.where(strict, logarithmic_retention, 0.0)
    suffix = lax.cumsum(logarithmic_retention, axis=2, reverse=True) - logarithmic_retention
    log_weight = jax.nn.log_sigmoid(scores) + suffix + keep_total[:, :, None]
    if is_own:
        log_weight = jnp.where(strict, log_weight, -jnp.inf)
    weights = jnp.where(is_valid, jnp.exp(log_weight), 0.0).astype(jnp.bfloat16)
    weighted = weighted + jnp.einsum(
        "hts,shd->thd", weights, key_value[1], preferred_element_type=jnp.float32
    )
    keep_total = keep_total + jnp.where(is_valid, jnp.sum(logarithmic_retention, axis=2), 0.0)
    return (weighted, keep_total)


def contract_rows(rows_in, weight):
    return lax.dot_general(
        rows_in, weight, (((1,), (1,)), ((), ())), preferred_element_type=jnp.float32
    )


def on_device(
    input_layer_rows,
    input_norm_gain,
    query_weight_attention,
    key_weight_attention,
    value_weight_attention,
    query_weight_recurrent,
    forget_weight_recurrent,
    value_weight_recurrent,
    gate_weight_recurrent,
    output_weight_attention,
    emitted_projection_linear_scan,
    score_offset,
    attention_norm_gain,
    recurrence_norm_gain,
    forget_floor,
    forget_offset,
    extra_log_decay,
):
    values = input_layer_rows[0].astype(jnp.float32)
    square_mean = jnp.mean(values * values, axis=-1, keepdims=True)
    normed = (values * lax.rsqrt(square_mean + epsilon) * input_norm_gain).astype(jnp.bfloat16)
    tokens = normed.shape[0]
    weights_in = (
        query_weight_attention,
        key_weight_attention,
        value_weight_attention,
        query_weight_recurrent,
        forget_weight_recurrent,
        value_weight_recurrent,
        gate_weight_recurrent,
    )
    pieces = (
        lax.all_gather(weights_in[0], ("sp", "fs"), axis=0, tiled=True),
        lax.all_gather(weights_in[1], ("sp", "fs"), axis=0, tiled=True),
        lax.all_gather(weights_in[2], ("sp", "fs"), axis=0, tiled=True),
        lax.all_gather(weights_in[3], ("sp", "fs"), axis=0, tiled=True),
        lax.all_gather(weights_in[4], ("sp", "fs"), axis=0, tiled=True),
        lax.all_gather(weights_in[5], ("sp", "fs"), axis=0, tiled=True),
        lax.all_gather(weights_in[6], ("sp", "fs"), axis=0, tiled=True),
    )
    projected = tuple(
        (jnp.dot(normed, weight, preferred_element_type=jnp.float32) for weight in pieces)
    )
    query_a, key_a, value_a, query_b, forget_b, input_b, gate_b = [
        column_block.astype(jnp.bfloat16) for column_block in projected
    ]
    out_a, out_b = (
        lax.all_gather(output_weight_attention, ("sp", "fs"), axis=0, tiled=True),
        lax.all_gather(emitted_projection_linear_scan, ("sp", "fs"), axis=0, tiled=True),
    )
    head_count = query_a.shape[1] // HEAD
    queries = query_a.reshape(tokens, head_count, HEAD)
    key_value = jnp.stack(
        [key_a.reshape(tokens, head_count, HEAD), value_a.reshape(tokens, head_count, HEAD)]
    )
    weighted = jnp.zeros((tokens, head_count, HEAD), jnp.float32)
    keep_total = jnp.zeros((head_count, tokens), jnp.float32)
    weighted, keep_total = stick_piece(
        queries, score_offset, weighted, keep_total, key_value, True, True
    )
    position = lax.axis_index("sp")
    seq_devices = lax.axis_size("sp")
    gathered = lax.all_gather(key_value, "sp", axis=1, tiled=True)

    def gathered_turn(turn_index, carried_state):
        weighted_now, keep_now = carried_state
        source = jnp.maximum(position - turn_index, 0) * tokens
        piece_pair = lax.dynamic_slice_in_dim(gathered, source, tokens, 1)
        return stick_piece(
            queries, score_offset, weighted_now, keep_now, piece_pair, False, position >= turn_index
        )

    weighted, keep_total = lax.fori_loop(1, seq_devices, gathered_turn, (weighted, keep_total))
    row_log_total = jnp.log(jnp.maximum(-jnp.expm1(keep_total), log_floor))[None]
    mixed_a = (
        head_norm(weighted, attention_norm_gain.reshape(head_count, HEAD))
        .reshape(tokens, head_count * HEAD)
        .astype(jnp.bfloat16)
    )
    forget_logits = forget_b.astype(jnp.float32) + forget_offset
    forget_log_value = (
        jnp.logaddexp(
            jnp.log(forget_floor), jnp.log1p(-forget_floor) + jax.nn.log_sigmoid(forget_logits)
        )
        + extra_log_decay[0]
    )
    key_in = (1.0 - forget_floor) * jax.nn.sigmoid(-forget_logits)
    query_rows_input = jax.nn.silu(query_b.astype(jnp.float32)).reshape(tokens, head_count, HEAD)
    value_in = input_b.astype(jnp.float32)
    fading_channel_groups = forget_log_value.reshape(tokens, head_count, HEAD)
    shaped = tuple(
        (
            array_in.reshape(tokens // BLOCK, BLOCK, head_count, HEAD)
            for array_in in (query_rows_input, forget_log_value, key_in, value_in)
        )
    )
    empty_state = jnp.zeros((head_count, HEAD, HEAD), jnp.float32)
    nearby_hidden_vector, local_out = lax.scan(recurrence_block, empty_state, shaped)
    local_out = local_out.reshape(tokens, head_count, HEAD)
    through = jnp.exp(jnp.sum(fading_channel_groups, axis=0))

    def chain_states(earlier, later):
        return (earlier[0] * later[0], later[0][:, :, None] * earlier[1] + later[1])

    identity = (jnp.ones_like(through), jnp.zeros_like(nearby_hidden_vector))
    unused_decay, incoming_state = entering(
        (through, nearby_hidden_vector), "sp", chain_states, identity
    )
    running_sum = jnp.cumsum(fading_channel_groups, axis=0)
    recurrent = local_out + jnp.einsum(
        "fby,bym->fbm",
        query_rows_input * jnp.exp(running_sum),
        incoming_state,
        precision=lax.Precision.HIGHEST,
    )
    gated_out = head_norm(recurrent, recurrence_norm_gain.reshape(head_count, HEAD)) * jax.nn.silu(
        gate_b.astype(jnp.float32).reshape(tokens, head_count, HEAD)
    )
    mixed_b = gated_out.reshape(tokens, head_count * HEAD).astype(jnp.bfloat16)
    summed = lax.psum_scatter(
        (contract_rows(mixed_a, out_a) + contract_rows(mixed_b, out_b)).astype(jnp.bfloat16),
        "tp",
        scatter_dimension=0,
        tiled=True,
    )
    layer_out = summed[None]
    return (layer_out, row_log_total)


def solution(mesh):
    return jax.shard_map(
        on_device,
        mesh=mesh,
        in_specs=(
            P("fs", "sp", None),
            P(),
            P(("sp", "fs"), "tp"),
            P(("sp", "fs"), "tp"),
            P(("sp", "fs"), "tp"),
            P(("sp", "fs"), "tp"),
            P(("sp", "fs"), "tp"),
            P(("sp", "fs"), "tp"),
            P(("sp", "fs"), "tp"),
            P(("sp", "fs"), "tp"),
            P(("sp", "fs"), "tp"),
            P("tp"),
            P("tp"),
            P("tp"),
            P("tp"),
            P("tp"),
            P("fs", "sp", "tp"),
        ),
        out_specs=(P("fs", ("sp", "tp"), None), P("fs", "tp", "sp")),
        check_vma=False,
    )
```

profile of v0, /device:TPU:0, one launch (start us, length us, event | category | flops | bytes accessed | tf_op | source)
XLA Modules:
  0.0 472.7 jit_solution(9286617565874748095)
XLA Ops:
  11.9 1.5 fusion.32
  13.5 40.9 %all-gather.16.cloned.1.call-done = bf16[2048,512]{1,0:T(8,128)(2,1)} async-done(((bf16[128,512]{1,0:T(8,128)(2,1)}), bf16[2048,512]{1,0:T(8,128)(2,1)}) %all-gather.16.cloned.1.call-update) | async-done | bytes 2097168 | tf_op jit(solution)/shard_map/all_gather | solution.py:130
  54.3 2.7 convolution_convert_fusion.4
  57.8 38.9 %all-gather.12.cloned.1.call-done = bf16[2048,512]{1,0:T(8,128)(2,1)} async-done(((bf16[128,512]{1,0:T(8,128)(2,1)}), bf16[2048,512]{1,0:T(8,128)(2,1)}) %all-gather.12.cloned.1.call-update) | async-done | bytes 2097168 | tf_op jit(solution)/shard_map/all_gather | solution.py:131
  96.7 2.3 convolution_convert_fusion.6
  102.2 36.9 %all-gather.22.cloned.1.call-done = bf16[2048,512]{1,0:T(8,128)(2,1)} async-done(((bf16[128,512]{1,0:T(8,128)(2,1)}), bf16[2048,512]{1,0:T(8,128)(2,1)}) %all-gather.22.cloned.1.call-update) | async-done | bytes 2097168 | tf_op jit(solution)/shard_map/all_gather | solution.py:133
  139.1 3.1 fusion.67
  143.6 37.7 %all-gather.26.cloned.1.call-done = bf16[2048,512]{1,0:T(8,128)(2,1)} async-done(((bf16[128,512]{1,0:T(8,128)(2,1)}), bf16[2048,512]{1,0:T(8,128)(2,1)}) %all-gather.26.cloned.1.call-update) | async-done | bytes 2097168 | tf_op jit(solution)/shard_map/all_gather | solution.py:132
  181.3 2.8 divide_multiply_fusion
  184.3 39.2 %all-gather.24.cloned.1.call-done = bf16[2048,512]{1,0:T(8,128)(2,1)} async-done(((bf16[128,512]{1,0:T(8,128)(2,1)}), bf16[2048,512]{1,0:T(8,128)(2,1)}) %all-gather.24.cloned.1.call-update) | async-done | bytes 2097168 | tf_op jit(solution)/shard_map/all_gather | solution.py:134
  223.5 2.7 fusion.39
  226.4 24.0 %while.43 = (s32[]{:T(128)}, f32[4,128,128]{2,1,0:T(8,128)S(1)}, f32[4,64,4,128]{3,1,0,2:T(8,128)}, f32[4,64,4,128]{3,2,1,0:T(4,128)S(1)}, f32[4,64,4,128]{3,2,1...) while((s32[]{:T(128)}, f32[4,128,128]{2,1,0:T(8,128)S(1)}, ...), condition=%wide.region_13.14_spmd.clone, body=%wide.region_10.13_spmd.clone.sunk | while | flops 138760192 | bytes 4346484 | solution.py:194
  226.7 3.7 multiply_reduce_fusion.4
  230.7 1.0 fusion.118
  232.7 3.7 multiply_reduce_fusion.4
  236.7 1.0 fusion.118
  238.7 3.7 multiply_reduce_fusion.4
  242.7 1.0 fusion.118
  244.7 3.7 multiply_reduce_fusion.4
  248.7 1.0 fusion.118
  250.5 20.1 %all-gather = bf16[16,128,128]{2,1,0:T(8,128)(2,1)S(1)} all-gather(bf16[4,128,128]{2,1,0:T(8,128)(2,1)S(1)} %convert_element_type.119), channel_id=2, replica_groups=mesh['sp'=4,'fs'=4,'tp'=2] {'sp'}, dimensions={0}, use_global_device_ids=true | all-gather | bytes 655360 | tf_op jit(solution)/shard_map/all_gather | solution.py:15
  270.6 9.2 %all_gather.48 = bf16[4,4,128]{2,1,0:T(4,128)(2,1)S(1)} all-gather(bf16[1,4,128]{2,1,0:T(4,128)(2,1)S(1)} %fusion.58), channel_id=1, replica_groups=mesh['sp'=4,'fs'=4,'tp'=2] {'sp'}, dimensions={0}, use_global_device_ids=true | all-gather | bytes 5120 | tf_op jit(solution)/shard_map/all_gather | solution.py:15
  279.8 12.2 %while.44 = (s32[]{:T(128)}, f32[4,128,128]{2,1,0:T(8,128)S(1)}, s32[]{:T(128)}, bf16[4,4,128]{2,1,0:T(4,128)(2,1)S(1)}, bf16[4,4,128,128]{3,2,1,0:T(8,128)(2,1)S(1)}, /*index=5*/s32[]{:T(128)}, s32[]{:T(128)}) while((s32[]{:T(128)}, f32[4,128,128]{2,1,0:T(8,128)S(1)}, s32[]{:T(128)}, bf16[4,4,128]{2,1,0:T(4,128)(2,1)S(1)}, ...), condition=%wide.region_16.17_spmd.clone, body=%wide.region_15.16_spmd.clone.sunk | while | flops 328196 | bytes 660585 | solution.py:32
  293.0 1.5 multiply_reduce_fusion.1
  294.5 2.5 fusion.41
  297.3 14.6 %all-gather.14.cloned.1.call-done = bf16[2048,512]{1,0:T(8,128)(2,1)} async-done(((bf16[128,512]{1,0:T(8,128)(2,1)}), bf16[2048,512]{1,0:T(8,128)(2,1)}) %all-gather.14.cloned.1.call-update) | async-done | bytes 2097168 | tf_op jit(solution)/shard_map/all_gather | solution.py:129
  311.9 2.3 fusion.42
  316.2 9.2 %fusion.48 = f32[4,256,2,128]{1,2,3,0:T(2,128)S(1)} fusion(f32[4,256,2,128]{1,3,2,0:T(8,128)S(1)} %bitcast.197), kind=kOutput, calls=%fused_computation.90 | output fusion | flops 33292288 | bytes 2097152 | tf_op jit(solution)/shard_map/reduce-window
  325.9 1.5 fusion.47
  327.7 0.9 multiply_convert_fusion
  328.6 29.9 %all-gather.18.cloned.1.call-done = bf16[2,1024,4,128]{3,1,2,0:T(8,128)(2,1)} async-done(((bf16[2,256,4,128]{3,1,2,0:T(8,128)(2,1)}), bf16[2,1024,4,128]{3,1,2,0:T(8,128)(2,1)}) %all-gather.18.cloned.1.call-update) | async-done | bytes 2097168 | tf_op jit(solution)/shard_map/all_gather | solution.py:159
  358.5 43.2 %while.42 = (s32[]{:T(128)}, f32[256,4,128]{0,2,1:T(8,128)S(1)}, f32[4,256]{1,0:T(4,128)S(1)}, s32[]{:T(128)}, bf16[2,1024,4,128]{3,1,2,0:T(8,128)(2,1)}, /*inde...) while((s32[]{:T(128)}, f32[256,4,128]{0,2,1:T(8,128)S(1)}, ...), condition=%wide.region_8.9_spmd, body=%wide.region_4.8_spmd.sunk | while | flops 175772672 | bytes 13451514 | solution.py:169
  358.5 1.9 fusion.107
  360.4 9.2 %fusion.108 = f32[4,256,2,128]{1,2,3,0:T(2,128)S(1)} fusion(f32[4,256,2,128]{1,3,2,0:T(8,128)S(1)} %bitcast.196), kind=kOutput, calls=%fused_computation.14.clone.1 | output fusion | flops 33292288 | bytes 2097152 | tf_op jit(solution)/shard_map/reduce-window.8
  370.1 1.4 fusion.109
  371.5 1.3 fusion.110
  372.9 1.9 fusion.107
  374.8 9.2 %fusion.108 = f32[4,256,2,128]{1,2,3,0:T(2,128)S(1)} fusion(f32[4,256,2,128]{1,3,2,0:T(8,128)S(1)} %bitcast.196), kind=kOutput, calls=%fused_computation.14.clone.1 | output fusion | flops 33292288 | bytes 2097152 | tf_op jit(solution)/shard_map/reduce-window.8
  384.5 1.4 fusion.109
  385.9 1.3 fusion.110
  387.3 1.9 fusion.107
  389.2 9.2 %fusion.108 = f32[4,256,2,128]{1,2,3,0:T(2,128)S(1)} fusion(f32[4,256,2,128]{1,3,2,0:T(8,128)S(1)} %bitcast.196), kind=kOutput, calls=%fused_computation.14.clone.1 | output fusion | flops 33292288 | bytes 2097152 | tf_op jit(solution)/shard_map/reduce-window.8
  398.9 1.4 fusion.109
  400.3 1.3 fusion.110
  401.9 2.4 fusion.68
  404.3 38.9 %all-gather.30.cloned.1.call-done = bf16[2048,512]{1,0:T(8,128)(2,1)} async-done(((bf16[128,512]{1,0:T(8,128)(2,1)}), bf16[2048,512]{1,0:T(8,128)(2,1)}) %all-gather.30.cloned.1.call-update) | async-done | bytes 2097168 | tf_op jit(solution)/shard_map/all_gather | solution.py:145
  443.2 3.3 fusion.31
  447.2 18.6 %reduce-scatter.2.cloned.1.call-done = bf16[128,2048]{1,0:T(8,128)(2,1)} async-done(((bf16[256,2048]{1,0:T(8,128)(2,1)}), bf16[128,2048]{1,0:T(8,128)(2,1)}) %reduce-scatter.2.cloned.1.call-update) | async-done | bytes 524304 | tf_op jit(solution)/shard_map/reduce_scatter | solution.py:216
  (165 shorter events, 21.9 us)
Async XLA Ops:
  7.2 47.2 %all-gather.16.cloned.1.call-start = ((), (), s32[]{:S(2)}) async-start(), calls=%async_computation.3 | async-start | bytes 2228224 | tf_op jit(solution)/shard_map/all_gather | solution.py:130
  7.9 88.8 %all-gather.12.cloned.1.call-start = ((), (), s32[]{:S(2)}) async-start(), calls=%async_computation.1 | async-start | bytes 2228224 | tf_op jit(solution)/shard_map/all_gather | solution.py:131
  8.6 130.4 %all-gather.22.cloned.1.call-start = ((), (), s32[]{:S(2)}) async-start(), calls=%async_computation.6 | async-start | bytes 2228224 | tf_op jit(solution)/shard_map/all_gather | solution.py:133
  9.4 171.9 %all-gather.26.cloned.1.call-start = ((), (), s32[]{:S(2)}) async-start(), calls=%async_computation.8 | async-start | bytes 2228224 | tf_op jit(solution)/shard_map/all_gather | solution.py:132
  10.0 213.6 %all-gather.24.cloned.1.call-start = ((), (), s32[]{:S(2)}) async-start(), calls=%async_computation.7 | async-start | bytes 2228224 | tf_op jit(solution)/shard_map/all_gather | solution.py:134
  10.5 284.0 %all-gather.28.cloned.1.call-start = ((), (), s32[]{:S(2)}) async-start(), calls=%async_computation.9 | async-start | bytes 2228224 | tf_op jit(solution)/shard_map/all_gather | solution.py:135
  11.1 300.8 %all-gather.14.cloned.1.call-start = ((), (), s32[]{:S(2)}) async-start(), calls=%async_computation.2 | async-start | bytes 2228224 | tf_op jit(solution)/shard_map/all_gather | solution.py:129
  11.9 346.6 %all-gather.18.cloned.1.call-start = ((), (), s32[]{:S(2)}) async-start(), calls=%async_computation.4 | async-start | bytes 2621440 | tf_op jit(solution)/shard_map/all_gather | solution.py:159
  13.4 83.3 %copy-start.4 = (bf16[1,256,2048]{2,1,0:T(8,128)(2,1)S(1)}, bf16[1,256,2048]{2,1,0:T(8,128)(2,1)}, u32[]{:S(2)}) copy-start(bf16[1,256,2048]{2,1,0:T(8,128)(2,1)} %param.23) | copy-start | bytes 3145732
  13.5 83.3 %copy-start.14 = (f32[2048]{0:T(1024)S(1)}, f32[2048]{0:T(1024)}, u32[]{:S(2)}) copy-start(f32[2048]{0:T(1024)} %param.24) | copy-start | bytes 24580
  57.0 0.7 copy-start.9
  99.1 3.1 copy-start.13
  99.1 40.0 %copy-start.15 = (f32[512]{0:T(512)S(1)}, f32[512]{0:T(512)}, u32[]{:S(2)}) copy-start(f32[512]{0:T(512)} %param.38) | copy-start | bytes 6148
  100.1 301.8 %all-gather.20.cloned.1.call-start = ((), (), s32[]{:S(2)}) async-start(), calls=%async_computation.5 | async-start | bytes 2228224 | tf_op jit(solution)/shard_map/all_gather | solution.py:144
  100.8 342.4 %all-gather.30.cloned.1.call-start = ((), (), s32[]{:S(2)}) async-start(), calls=%async_computation.10 | async-start | bytes 2228224 | tf_op jit(solution)/shard_map/all_gather | solution.py:145
  101.4 364.4 %reduce-scatter.2.cloned.1.call-start = ((), (), s32[]{:S(2)}) async-start(), calls=%async_computation.11 | async-start | bytes 1572864 | tf_op jit(solution)/shard_map/reduce_scatter | solution.py:216
  184.1 39.4 %copy-start.2 = (f32[256,512]{1,0:T(8,128)}, f32[256,512]{1,0:T(8,128)S(1)}, u32[]{:S(2)}) copy-start(f32[256,512]{1,0:T(8,128)S(1)} %divide_multiply_fusion) | copy-start | bytes 1572868
  250.5 41.5 %copy-start.8 = (f32[4,64,4,128]{3,1,0,2:T(8,128)S(1)}, f32[4,64,4,128]{3,1,0,2:T(8,128)}, u32[]{:S(2)}) copy-start(f32[4,64,4,128]{3,1,0,2:T(8,128)} %get-tuple-element.260) | copy-start | bytes 1572868
  279.8 12.4 %copy-start = (f32[256,4,128]{2,0,1:T(8,128)S(1)}, f32[256,4,128]{2,0,1:T(8,128)}, u32[]{:S(2)}) copy-start(f32[256,4,128]{2,0,1:T(8,128)} %copy_bitcast_fusion.3) | copy-start | bytes 1572868
  292.0 1.0 copy-start.3
  292.8 1.8 copy-start.5
  297.3 17.8 %copy-start.10 = (bf16[256,512]{1,0:T(8,128)(2,1)S(1)}, bf16[256,512]{1,0:T(8,128)(2,1)}, u32[]{:S(2)}) copy-start(bf16[256,512]{1,0:T(8,128)(2,1)} %copy-done.9) | copy-start | bytes 786436
  297.3 17.7 %copy-start.16 = (f32[4]{0:T(128)S(1)}, f32[4]{0:T(128)}, u32[]{:S(2)}) copy-start(f32[4]{0:T(128)} %param.34) | copy-start | bytes 52
  314.3 1.1 copy-start.7
  325.9 1.7 copy-start.1
  325.9 1.7 copy-start.11
  358.5 43.2 %copy-start.12 = (f32[512]{0:T(512)S(1)}, f32[512]{0:T(512)}, u32[]{:S(2)}) copy-start(f32[512]{0:T(512)} %param.35) | copy-start | bytes 6148
  401.9 41.3 %copy-start.6 = (bf16[256,4,128]{0,2,1:T(8,128)(2,1)S(1)}, bf16[256,4,128]{0,2,1:T(8,128)(2,1)}, u32[]{:S(2)}) copy-start(bf16[256,4,128]{0,2,1:T(8,128)(2,1)} %multiply_convert_fusion) | copy-start | bytes 786436
Sparse Core Ops, SparseCore 0:
  10.1 44.1 all-gather.15
  56.5 40.1 all-gather.11
  98.9 40.1 all-gather.21
  141.1 40.1 all-gather.25
  183.3 40.1 all-gather.23
  225.5 43.2 all-gather.27
  271.0 40.8 all-gather.13
  314.1 44.3 all-gather.17
  360.6 40.3 all-gather.19
  403.0 40.1 all-gather.29
  446.7 19.0 reduce-scatter.1
where the time goes:
time: 480 us; the launch traced here: 473 us
  waiting for transfers between devices  301 us (63%)
  other arithmetic  66.7 us (14%)
  matrix products  43.6 us (9%)
  blocking collectives  29.3 us (6%)
  between operations  14.7 us (3%)
  loops' own time  11.9 us (2%)
    all_gather x1, waiting for transfers between devices, on_device(): lax.all_gather(weights_in[1], ('sp', 'fs'), axis=0, tiled=True)  40.9 us
    all_gather x1, waiting for transfers between devices, on_device(): lax.all_gather(weights_in[5], ('sp', 'fs'), axis=0, tiled=True)  39.2 us
    all_gather x1, waiting for transfers between devices, on_device(): lax.all_gather(emitted_projection_linear_scan, ('sp', 'fs'), axis=0, tile...  38.9 us
    all_gather x1, waiting for transfers between devices, on_device(): lax.all_gather(weights_in[2], ('sp', 'fs'), axis=0, tiled=True)  38.9 us
    all_gather x1, waiting for transfers between devices, on_device(): lax.all_gather(weights_in[3], ('sp', 'fs'), axis=0, tiled=True)  37.7 us
    another operation x10, other arithmetic  37.4 us
    all_gather x1, waiting for transfers between devices, on_device(): lax.all_gather(weights_in[4], ('sp', 'fs'), axis=0, tiled=True)  36.9 us
    all_gather x1, waiting for transfers between devices, on_device(): gathered = lax.all_gather(key_value, 'sp', axis=1, tiled=True)  29.9 us
  transfers between devices with their start and end apart: 11, of which 9 were waited for; matrix products, arithmetic and copies ran while one was open for 23% of the time, Pallas kernels for 0%

commit v1 on v0

--- a/solution.py
+++ b/solution.py
@@ -156,7 +156,16 @@
     )
     position = lax.axis_index("sp")
     seq_devices = lax.axis_size("sp")
-    gathered = lax.all_gather(key_value, "sp", axis=1, tiled=True)
+    num_devices = jax.lax.axis_size("sp")
+    z2 = [None] * num_devices
+    z2[num_devices - 1] = key_value
+    blocks_here = [(ii, (ii + 1) % num_devices) for ii in range(num_devices)]
+    for u in range(num_devices - 2, -1, -1):
+        z2[u] = jax.lax.ppermute(z2[u + 1], "sp", blocks_here)
+    val2 = jnp.concatenate(z2, axis=1)
+    side_arr = jax.lax.axis_index("sp")
+    front = (side_arr + 1) * key_value.shape[1]
+    gathered = jnp.roll(val2, front, axis=1)
 
     def gathered_turn(turn_index, carried_state):
         weighted_now, keep_now = carried_state

time: 480 us -> 453 us (0.944)
  waiting for transfers between devices: 301 us -> 268 us
  local copies, waits for them, and re-layouts: 4.66 us -> 16.5 us
  loops' own time: 11.9 us -> 0.85 us
  other arithmetic: 66.7 us -> 74.4 us
    all_gather x1, waiting for transfers between devices: 38.9 us -> 0.02 us  [on_device(): lax.all_gather(emitted_projection_linear_scan, ('sp', 'fs'), axis=0, tile...]
    all_gather x1 -> x0, waiting for transfers between devices: 29.9 us -> none  [on_device(): gathered = lax.all_gather(key_value, 'sp', axis=1, tiled=True)]
    all_gather x1, waiting for transfers between devices: 14.6 us -> 40.7 us  [on_device(): lax.all_gather(weights_in[0], ('sp', 'fs'), axis=0, tiled=True)]
    ppermute x0 -> x3, waiting for transfers between devices: none -> 24.2 us  [on_device(): z2[u] = jax.lax.ppermute(z2[u + 1], 'sp', blocks_here)]
    all_gather x1, waiting for transfers between devices: 37.7 us -> 25.8 us  [on_device(): lax.all_gather(weights_in[3], ('sp', 'fs'), axis=0, tiled=True)]
    another operation x1, loops' own time: 11.4 us -> 0.12 us  [entering(): return lax.fori_loop(0, size, hop, start)]
  transfers between devices with their start and end apart: 11 -> 13, of which waited for: 9 -> 9; matrix products, arithmetic and copies ran while one was open for 23% -> 30% of each run, Pallas kernels for 0% -> 0%
where the time goes in v1:
time: 453 us; the launch traced here: 449 us
  waiting for transfers between devices  268 us (59%)
  other arithmetic  74.4 us (16%)
  matrix products  46 us (10%)
  blocking collectives  25.9 us (6%)
  local copies, waits for them, and re-layouts  16.5 us (4%)
  between operations  15 us (3%)
    all_gather x1, waiting for transfers between devices, on_device(): lax.all_gather(weights_in[0], ('sp', 'fs'), axis=0, tiled=True)  40.7 us
    all_gather x1, waiting for transfers between devices, on_device(): lax.all_gather(weights_in[2], ('sp', 'fs'), axis=0, tiled=True)  39.9 us
    all_gather x1, waiting for transfers between devices, on_device(): lax.all_gather(weights_in[4], ('sp', 'fs'), axis=0, tiled=True)  39.3 us
    all_gather x1, waiting for transfers between devices, on_device(): lax.all_gather(weights_in[5], ('sp', 'fs'), axis=0, tiled=True)  38.5 us
    another operation x10, other arithmetic  37.4 us
    all_gather x1, waiting for transfers between devices, on_device(): lax.all_gather(weights_in[1], ('sp', 'fs'), axis=0, tiled=True)  36.7 us
    all_gather x2, blocking collectives, entering(): lax.all_gather(part.astype(kind), axis)  25.9 us
    all_gather x1, waiting for transfers between devices, on_device(): lax.all_gather(weights_in[3], ('sp', 'fs'), axis=0, tiled=True)  25.8 us
  transfers between devices with their start and end apart: 13, of which 9 were waited for; matrix products, arithmetic and copies ran while one was open for 30% of the time, Pallas kernels for 0%

profile of v1, /device:TPU:0, one launch (start us, length us, event | category | flops | bytes accessed | tf_op | source)
XLA Modules:
  0.0 448.8 jit_solution(475462669756955969)
XLA Ops:
  13.5 1.5 fusion.32
  15.1 39.3 %all-gather.19.cloned.1.call-done = bf16[2048,512]{1,0:T(8,128)(2,1)} async-done(((bf16[128,512]{1,0:T(8,128)(2,1)}), bf16[2048,512]{1,0:T(8,128)(2,1)}) %all-gather.19.cloned.1.call-update) | async-done | bytes 2097168 | tf_op jit(solution)/shard_map/all_gather | solution.py:133
  54.4 3.8 fusion.67
  60.1 36.7 %all-gather.15.cloned.1.call-done = bf16[2048,512]{1,0:T(8,128)(2,1)} async-done(((bf16[128,512]{1,0:T(8,128)(2,1)}), bf16[2048,512]{1,0:T(8,128)(2,1)}) %all-gather.15.cloned.1.call-update) | async-done | bytes 2097168 | tf_op jit(solution)/shard_map/all_gather | solution.py:130
  96.8 2.3 convolution_convert_fusion.4
  99.2 39.9 %all-gather.11.cloned.1.call-done = bf16[2048,512]{1,0:T(8,128)(2,1)} async-done(((bf16[128,512]{1,0:T(8,128)(2,1)}), bf16[2048,512]{1,0:T(8,128)(2,1)}) %all-gather.11.cloned.1.call-update) | async-done | bytes 2097168 | tf_op jit(solution)/shard_map/all_gather | solution.py:131
  139.1 2.3 convolution_convert_fusion.6
  143.3 40.7 %all-gather.13.cloned.1.call-done = bf16[2048,512]{1,0:T(8,128)(2,1)} async-done(((bf16[128,512]{1,0:T(8,128)(2,1)}), bf16[2048,512]{1,0:T(8,128)(2,1)}) %all-gather.13.cloned.1.call-update) | async-done | bytes 2097168 | tf_op jit(solution)/shard_map/all_gather | solution.py:129
  183.9 2.3 fusion.42
  186.3 1.4 fusion.55
  188.5 9.2 %fusion.48 = f32[4,256,2,128]{1,2,3,0:T(2,128)S(1)} fusion(f32[4,256,2,128]{1,3,2,0:T(8,128)S(1)} %bitcast.197), kind=kOutput, calls=%fused_computation.90 | output fusion | flops 33292288 | bytes 2097152 | tf_op jit(solution)/shard_map/reduce-window
  199.2 1.2 reshape.161
  200.4 25.8 %all-gather.23.cloned.1.call-done = bf16[2048,512]{1,0:T(8,128)(2,1)} async-done(((bf16[128,512]{1,0:T(8,128)(2,1)}), bf16[2048,512]{1,0:T(8,128)(2,1)}) %all-gather.23.cloned.1.call-update) | async-done | bytes 2097168 | tf_op jit(solution)/shard_map/all_gather | solution.py:132
  226.2 2.8 divide_multiply_fusion
  229.9 38.5 %all-gather.21.cloned.1.call-done = bf16[2048,512]{1,0:T(8,128)(2,1)} async-done(((bf16[128,512]{1,0:T(8,128)(2,1)}), bf16[2048,512]{1,0:T(8,128)(2,1)}) %all-gather.21.cloned.1.call-update) | async-done | bytes 2097168 | tf_op jit(solution)/shard_map/all_gather | solution.py:134
  268.4 2.7 fusion.39
  271.3 31.5 %while.43 = (s32[]{:T(128)}, f32[4,128,128]{2,1,0:T(8,128)S(1)}, f32[4,64,4,128]{3,1,0,2:T(8,128)}, f32[4,64,4,128]{3,2,1,0:T(4,128)}, f32[4,64,4,128]{3,2,1,0:T...) while((s32[]{:T(128)}, f32[4,128,128]{2,1,0:T(8,128)S(1)}, ...), condition=%wide.region_13.14_spmd.clone, body=%wide.region_10.13_spmd.clone.sunk | while | flops 138760192 | bytes 4346992 | solution.py:203
  273.4 3.7 multiply_reduce_fusion.4
  281.3 3.7 multiply_reduce_fusion.4
  289.2 3.7 multiply_reduce_fusion.4
  297.0 3.7 multiply_reduce_fusion.4
  302.8 16.8 %all-gather = bf16[16,128,128]{2,1,0:T(8,128)(2,1)S(1)} all-gather(bf16[4,128,128]{2,1,0:T(8,128)(2,1)S(1)} %convert_element_type.119), channel_id=2, replica_groups=mesh['sp'=4,'fs'=4,'tp'=2] {'sp'}, dimensions={0}, use_global_device_ids=true | all-gather | bytes 655360 | tf_op jit(solution)/shard_map/all_gather | solution.py:15
  319.7 9.1 %all_gather.44 = bf16[4,4,128]{2,1,0:T(4,128)(2,1)S(1)} all-gather(bf16[1,4,128]{2,1,0:T(4,128)(2,1)S(1)} %fusion.58), channel_id=1, replica_groups=mesh['sp'=4,'fs'=4,'tp'=2] {'sp'}, dimensions={0}, use_global_device_ids=true | all-gather | bytes 5120 | tf_op jit(solution)/shard_map/all_gather | solution.py:15
  332.2 3.6 fusion.41
  337.2 2.3 fusion.47
  339.5 19.5 %collective-permute-done.1 = bf16[2,256,4,128]{3,1,2,0:T(8,128)(2,1)S(1)} collective-permute-done((bf16[2,256,4,128]{3,1,2,0:T(8,128)(2,1)}, bf16[2,256,4,128]{3,1,2,0:T(8,128)(2,1)S(1)}, u32[]{:S(2)}, u32[]{:S(2)}) %collective-permute-start.1) | collective-permute-done | bytes 524320 | tf_op jit(solution)/shard_map/ppermute | solution.py:164
  360.1 1.7 copy.171
  361.8 1.2 copy.113
  363.1 1.3 convolution_bitcast_fusion.4
  365.2 4.7 %collective-permute-done.2 = bf16[2,256,4,128]{3,1,2,0:T(8,128)(2,1)S(1)} collective-permute-done((bf16[2,256,4,128]{3,1,2,0:T(8,128)(2,1)S(1)}, bf16[2,256,4,128]{3,1,2,0:T(8,128)(2,1)S(1)}, u32[]{:S(2)}, u32[]{:S(2)}) %collective-permute-start.2) | collective-permute-done | bytes 524320 | tf_op jit(solution)/shard_map/ppermute | solution.py:164
  370.1 1.1 constant_dynamic-update-slice_fusion.7
  372.8 1.5 constant_dynamic-slice_fusion.1
  374.3 43.1 %while.42 = (s32[]{:T(128)}, f32[256,4,128]{0,2,1:T(8,128)S(1)}, f32[4,256]{1,0:T(4,128)S(1)}, s32[]{:T(128)}, bf16[2,1024,4,128]{3,1,2,0:T(8,128)(2,1)}, /*inde...) while((s32[]{:T(128)}, f32[256,4,128]{0,2,1:T(8,128)S(1)}, ...), condition=%wide.region_8.9_spmd, body=%wide.region_4.8_spmd.sunk | while | flops 175772672 | bytes 13451514 | solution.py:178
  374.5 1.8 fusion.107
  376.3 9.2 %fusion.108 = f32[4,256,2,128]{1,2,3,0:T(2,128)S(1)} fusion(f32[4,256,2,128]{1,3,2,0:T(8,128)S(1)} %bitcast.196), kind=kOutput, calls=%fused_computation.14.clone.1 | output fusion | flops 33292288 | bytes 2097152 | tf_op jit(solution)/shard_map/reduce-window.8
  386.1 1.4 fusion.109
  387.5 1.3 fusion.110
  388.8 1.8 fusion.107
  390.6 9.2 %fusion.108 = f32[4,256,2,128]{1,2,3,0:T(2,128)S(1)} fusion(f32[4,256,2,128]{1,3,2,0:T(8,128)S(1)} %bitcast.196), kind=kOutput, calls=%fused_computation.14.clone.1 | output fusion | flops 33292288 | bytes 2097152 | tf_op jit(solution)/shard_map/reduce-window.8
  400.4 1.4 fusion.109
  401.8 1.3 fusion.110
  403.1 1.8 fusion.107
  405.0 9.2 %fusion.108 = f32[4,256,2,128]{1,2,3,0:T(2,128)S(1)} fusion(f32[4,256,2,128]{1,3,2,0:T(8,128)S(1)} %bitcast.196), kind=kOutput, calls=%fused_computation.14.clone.1 | output fusion | flops 33292288 | bytes 2097152 | tf_op jit(solution)/shard_map/reduce-window.8
  414.7 1.4 fusion.109
  416.1 1.3 fusion.110
  417.7 2.4 fusion.68
  420.1 3.3 fusion.31
  424.1 17.6 %reduce-scatter.2.cloned.1.call-done = bf16[128,2048]{1,0:T(8,128)(2,1)} async-done(((bf16[256,2048]{1,0:T(8,128)(2,1)}), bf16[128,2048]{1,0:T(8,128)(2,1)}) %reduce-scatter.2.cloned.1.call-update) | async-done | bytes 524304 | tf_op jit(solution)/shard_map/reduce_scatter | solution.py:225
  (199 shorter events, 41.2 us)
Async XLA Ops:
  7.2 47.2 %copy-start.6 = (bf16[1,256,2048]{2,1,0:T(8,128)(2,1)S(1)}, bf16[1,256,2048]{2,1,0:T(8,128)(2,1)}, u32[]{:S(2)}) copy-start(bf16[1,256,2048]{2,1,0:T(8,128)(2,1)} %param.23) | copy-start | bytes 3145732
  7.2 7.9 %copy-start.16 = (f32[512]{0:T(512)S(1)}, f32[512]{0:T(512)}, u32[]{:S(2)}) copy-start(f32[512]{0:T(512)} %param.37) | copy-start | bytes 6148
  7.2 47.2 %copy-start.21 = (f32[2048]{0:T(1024)S(1)}, f32[2048]{0:T(1024)}, u32[]{:S(2)}) copy-start(f32[2048]{0:T(1024)} %param.24) | copy-start | bytes 24580
  7.2 47.2 %copy-start.24 = (f32[512]{0:T(512)S(1)}, f32[512]{0:T(512)}, u32[]{:S(2)}) copy-start(f32[512]{0:T(512)} %param.38) | copy-start | bytes 6148
  7.2 47.2 %copy-start.20 = (f32[1,256,512]{2,1,0:T(8,128)S(1)}, f32[1,256,512]{2,1,0:T(8,128)}, u32[]{:S(2)}) copy-start(f32[1,256,512]{2,1,0:T(8,128)} %param.39) | copy-start | bytes 1572868
  7.2 47.2 %all-gather.19.cloned.1.call-start = ((), (), s32[]{:S(2)}) async-start(), calls=%async_computation.5 | async-start | bytes 2228224 | tf_op jit(solution)/shard_map/all_gather | solution.py:133
  8.0 88.8 %all-gather.15.cloned.1.call-start = ((), (), s32[]{:S(2)}) async-start(), calls=%async_computation.3 | async-start | bytes 2228224 | tf_op jit(solution)/shard_map/all_gather | solution.py:130
  8.7 130.4 %all-gather.11.cloned.1.call-start = ((), (), s32[]{:S(2)}) async-start(), calls=%async_computation.1 | async-start | bytes 2228224 | tf_op jit(solution)/shard_map/all_gather | solution.py:131
  9.4 174.5 %all-gather.13.cloned.1.call-start = ((), (), s32[]{:S(2)}) async-start(), calls=%async_computation.2 | async-start | bytes 2228224 | tf_op jit(solution)/shard_map/all_gather | solution.py:129
  10.0 216.1 %all-gather.23.cloned.1.call-start = ((), (), s32[]{:S(2)}) async-start(), calls=%async_computation.7 | async-start | bytes 2228224 | tf_op jit(solution)/shard_map/all_gather | solution.py:132
  10.6 257.8 %all-gather.21.cloned.1.call-start = ((), (), s32[]{:S(2)}) async-start(), calls=%async_computation.6 | async-start | bytes 2228224 | tf_op jit(solution)/shard_map/all_gather | solution.py:134
  11.2 321.0 %all-gather.25.cloned.1.call-start = ((), (), s32[]{:S(2)}) async-start(), calls=%async_computation.8 | async-start | bytes 2228224 | tf_op jit(solution)/shard_map/all_gather | solution.py:135
  11.9 405.8 %all-gather.17.cloned.1.call-start = ((), (), s32[]{:S(2)}) async-start(), calls=%async_computation.4 | async-start | bytes 2228224 | tf_op jit(solution)/shard_map/all_gather | solution.py:144
  12.7 407.4 %all-gather.27.cloned.1.call-start = ((), (), s32[]{:S(2)}) async-start(), calls=%async_computation.9 | async-start | bytes 2228224 | tf_op jit(solution)/shard_map/all_gather | solution.py:145
  13.4 428.3 %reduce-scatter.2.cloned.1.call-start = ((), (), s32[]{:S(2)}) async-start(), calls=%async_computation.10 | async-start | bytes 1572864 | tf_op jit(solution)/shard_map/reduce_scatter | solution.py:225
  15.1 168.8 %copy-start.17 = (f32[256]{0:T(256)}, f32[256]{0:T(256)S(1)}, u32[]{:S(2)}) copy-start(f32[256]{0:T(256)S(1)} %add_rsqrt_fusion.2) | copy-start | bytes 3076
  99.1 42.4 %copy-start.13 = (bf16[256,512]{1,0:T(8,128)(2,1)}, bf16[256,512]{1,0:T(8,128)(2,1)S(1)}, u32[]{:S(2)}) copy-start(bf16[256,512]{1,0:T(8,128)(2,1)S(1)} %convolution_convert_fusion.4) | copy-start | bytes 786436
  141.5 42.4 %copy-start.7 = (bf16[256,512]{1,0:T(8,128)(2,1)}, bf16[256,512]{1,0:T(8,128)(2,1)S(1)}, u32[]{:S(2)}) copy-start(bf16[256,512]{1,0:T(8,128)(2,1)S(1)} %convolution_convert_fusion.6) | copy-start | bytes 786436
  142.5 43.8 %copy-start.25 = (f32[4]{0:T(128)S(1)}, f32[4]{0:T(128)}, u32[]{:S(2)}) copy-start(f32[4]{0:T(128)} %param.34) | copy-start | bytes 52
  142.5 193.4 %collective-permute-start = (bf16[2,256,4,128]{3,1,2,0:T(8,128)(2,1)}, bf16[2,256,4,128]{3,1,2,0:T(8,128)(2,1)}, u32[]{:S(2)}, u32[]{:S(2)}) collective-permute-start(bf16[2,256,4,128]{3,1,2,0:T(8,128)(2,1)} %pad_maximum_fusion), channel_id=1, source_target_pairs={{0,8},{8,16},{16,24},{24,0},{1,9},{9,17},{17,25},{25,1},{2,10},{10... | collective-permute-start | bytes 1572872 | tf_op jit(solution)/shard_map/ppermute | solution.py:164
  186.3 11.4 %copy-start.11 = (bf16[32,4,8,128]{3,2,1,0:T(8,128)(2,1)}, bf16[32,4,8,128]{3,2,1,0:T(8,128)(2,1)S(1)}, u32[]{:S(2)}) copy-start(bf16[32,4,8,128]{3,2,1,0:T(8,128)(2,1)S(1)} %fusion.42) | copy-start | bytes 786436
  198.1 1.1 copy-start.10
  198.1 28.0 %copy-start.18 = (f32[256]{0:T(256)S(1)}, f32[256]{0:T(256)}, u32[]{:S(2)}) copy-start(f32[256]{0:T(256)} %copy-done.17) | copy-start | bytes 3076
  198.1 28.0 %copy-start.22 = (f32[2048]{0:T(1024)S(1)}, f32[2048]{0:T(1024)}, u32[]{:S(2)}) copy-start(f32[2048]{0:T(1024)} %param.24) | copy-start | bytes 24580
  228.9 39.5 %copy-start.2 = (f32[256,512]{1,0:T(8,128)}, f32[256,512]{1,0:T(8,128)S(1)}, u32[]{:S(2)}) copy-start(f32[256,512]{1,0:T(8,128)S(1)} %divide_multiply_fusion) | copy-start | bytes 1572868
  302.8 26.9 %copy-start.9 = (f32[4,64,4,128]{3,1,0,2:T(8,128)S(1)}, f32[4,64,4,128]{3,1,0,2:T(8,128)}, u32[]{:S(2)}) copy-start(f32[4,64,4,128]{3,1,0,2:T(8,128)} %get-tuple-element.260) | copy-start | bytes 1572868
  328.7 2.0 copy-start.1
  329.7 2.5 copy-start.19
  329.7 2.5 copy-start.23
  332.2 4.1 copy-start.3
  332.2 4.1 copy-start.4
  332.2 4.1 copy-start.5
  335.8 1.4 copy-start
  335.8 23.2 %collective-permute-start.1 = (bf16[2,256,4,128]{3,1,2,0:T(8,128)(2,1)}, bf16[2,256,4,128]{3,1,2,0:T(8,128)(2,1)S(1)}, u32[]{:S(2)}, u32[]{:S(2)}) collective-permute-start(bf16[2,256,4,128]{3,1,2,0:T(8,128)(2,1)} %collective-permute-done), channel_id=1, source_target_pairs={{0,8},{8,16},{16,24},{24,0},{1,9},{9,17},{17,25},{25,1},{2,10},{10... | collective-permute-start | bytes 1572872 | tf_op jit(solution)/shard_map/ppermute | solution.py:164
  339.5 24.8 %copy-start.14 = (f32[512]{0:T(512)S(1)}, f32[512]{0:T(512)}, u32[]{:S(2)}) copy-start(f32[512]{0:T(512)} %param.36) | copy-start | bytes 6148
  359.0 11.0 %collective-permute-start.2 = (bf16[2,256,4,128]{3,1,2,0:T(8,128)(2,1)S(1)}, bf16[2,256,4,128]{3,1,2,0:T(8,128)(2,1)S(1)}, u32[]{:S(2)}, u32[]{:S(2)}) collective-permute-start(bf16[2,256,4,128]{3,1,2,0:T(8,128)(2,1)S(1)} %collective-permute-done.1), channel_id=1, source_target_pairs={{0,8},{8,16},{16,24},{24,0},{1,9},{9,17},{17,25},{25,1},{2,10},{10... | collective-permute-start | bytes 1572872 | tf_op jit(solution)/shard_map/ppermute | solution.py:164
  372.8 1.5 copy-start.12
  372.8 1.5 copy-start.26
  374.3 43.2 %copy-start.15 = (f32[512]{0:T(512)S(1)}, f32[512]{0:T(512)}, u32[]{:S(2)}) copy-start(f32[512]{0:T(512)} %param.35) | copy-start | bytes 6148
  417.7 2.4 copy-start.8
Sparse Core Ops, SparseCore 0:
  10.2 44.1 all-gather.18
  56.6 40.1 all-gather.14
  98.9 40.1 all-gather.10
  141.2 42.7 all-gather.12
  185.9 40.1 all-gather.22
  228.2 40.1 all-gather.20
  270.5 41.0 all-gather.24
  313.8 48.9 all-gather.16
  365.0 38.7 all-gather.26
  423.6 18.0 reduce-scatter.1
